TPU v7x, 32 devices: a whole 2x2x4 slice. The times are simulated.
32 devices in a mesh: ep: 32 (over z, y, x, core).
Axes of the slice: x: 2, y: 2, z: 4, core: 2. Of those that a mesh axis runs over, the one named last changes fastest.
Arguments:
- tokens: bfloat16 [512, 2048], P('ep'), may hold values from -6 to 6
- lengths: int32 [512], P('ep'), may hold values from 1 to 1024, 262144 in all
- cache_keys: bfloat16 [512, 1024, 128], P('ep'), may hold values from -6 to 6
- cache_values: bfloat16 [512, 1024, 128], P('ep'), may hold values from -6 to 6
- mix_gain: float32 [2048], replicated, may hold values from 0.1 to 1.9
- mix_out_gain: float32 [2048], replicated, may hold values from 0.1 to 1.9
- ffn_gain: float32 [2048], replicated, may hold values from 0.1 to 1.9
- ffn_out_gain: float32 [2048], replicated, may hold values from 0.1 to 1.9
- query_weight: bfloat16 [2048, 2048], P(None, 'ep'), may hold values from -0.125 to 0.125
- key_weight: bfloat16 [2048, 128], replicated, may hold values from -0.125 to 0.125
- value_weight: bfloat16 [2048, 128], replicated, may hold values from -0.125 to 0.125
- head_bias: float32 [32], replicated, may hold values from -8 to -2
- output_weight: bfloat16 [2048, 2048], P(None, 'ep'), may hold values from -0.125 to 0.125
- routes: int32 [512, 6], P('ep'), may hold values from 0 to 31, all different within a row; in each aligned block of 16 rows (0 to 15, 16 to 31, ...) at most 6 rows name the same one
- route_weights: float32 [512, 6], P('ep'), may hold values from 0.1 to 1
- expert_gate: bfloat16 [32, 2048, 512], P('ep'), may hold values from -0.125 to 0.125
- expert_up: bfloat16 [32, 2048, 512], P('ep'), may hold values from -0.125 to 0.125
- expert_down: bfloat16 [32, 512, 2048], P('ep'), may hold values from -0.25 to 0.25
- shared_gate: bfloat16 [2048, 512], replicated, may hold values from -0.125 to 0.125
- shared_up: bfloat16 [2048, 512], replicated, may hold values from -0.125 to 0.125
- shared_down: bfloat16 [512, 2048], replicated, may hold values from -0.25 to 0.25
Outputs:
- layer_out: bfloat16 [512, 2048], P('ep')
- new_keys: bfloat16 [512, 128], P('ep')
- new_values: bfloat16 [512, 128], P('ep')
Inputs may be any that keep to these rules, and one draw needn't show every extreme that they name: `routes`: each row names 6 different experts. Among the rows of one device no expert is named more than 6 times, a bound that some block reaches in some device's rows. `lengths`: the new token stands at this position; cache entries at this position and after are unused. Some sequence has exactly 1024.
All inputs are finite; a program needn't handle non-finite values. No bound on the sum of `lengths` on one device may be relied on, other than what follows from the above.
Results may differ from a plain program's by a relative error of at most 0.013.
Values may be sent and summed in bfloat16 or wider, within the bound.
A program may use at most 128 MiB of HBM per device.

v0:
```python
import functools

import jax
import jax.numpy as jnp
from jax import lax
from jax.experimental import pallas as pl
from jax.experimental.pallas import tpu as pltpu
from jax.sharding import PartitionSpec as P

HD = 64
LANES = 128
F32 = jnp.float32
BF16 = jnp.bfloat16
Z_PER_GROUP = 2


def rms_scale(rows, gain):
    return rows * lax.rsqrt(jnp.mean(rows * rows, axis=-1, keepdims=True) + 1e-06) * gain


def dot(a, b):
    return jnp.dot(a, b, preferred_element_type=F32)


def loop(start, stop, one):
    def step(i, carry):
        one(i)
        return carry

    lax.fori_loop(start, stop, step, 0)


def remote(src, dst, send_sem, recv_sem, device):
    return pltpu.make_async_remote_copy(
        src_ref=src,
        dst_ref=dst,
        send_sem=send_sem,
        recv_sem=recv_sem,
        device_id=(device,),
        device_id_type=pl.DeviceIdType.MESH,
    )


class Place:
    def __init__(self, n):
        me = lax.axis_index("ep")
        self.n, self.lines = n, n // 4
        self.chip, self.core = me // 2, me % 2
        self.partner = 2 * self.chip + (1 - self.core)
        self.z, self.q = self.chip // 4, self.chip % 4
        self.qx = self.q + 1 - 2 * (self.q % 2)
        self.qy = self.q + 2 - 4 * (self.q // 2)
        self.qd = 3 - self.q

    def device(self, chip):
        return 2 * chip + self.core

    def back_z(self, i):
        return (self.z + self.lines - i) % self.lines


class Direct:
    def __init__(self, here, buf, send_sems, recv_sems):
        self.here, self.buf, self.send_sems, self.recv_sems = here, buf, send_sems, recv_sems

    def send(self, src, chip):
        here = self.here
        remote(
            src, self.buf.at[here.chip], self.send_sems.at[chip],
            self.recv_sems.at[here.chip], here.device(chip),
        ).start()

    def wait(self, chip):
        remote(
            self.buf.at[chip], self.buf.at[chip], self.send_sems.at[chip],
            self.recv_sems.at[chip], self.here.partner,
        ).wait_recv()

    def wait_sent(self, chip):
        remote(
            self.buf.at[chip], self.buf.at[chip], self.send_sems.at[chip],
            self.recv_sems.at[chip], self.here.partner,
        ).wait_send()

    def others(self, one):
        here = self.here
        loop(1, here.n, lambda i: one((here.chip + i) % here.n))


class Gather:
    def __init__(self, here, buf, send_sems, recv_sems):
        self.here, self.buf, self.send_sems, self.recv_sems = here, buf, send_sems, recv_sems

    def copy(self, src, slot, kind, index, chip):
        return remote(
            src, self.buf.at[slot], self.send_sems.at[kind, index],
            self.recv_sems.at[slot], self.here.device(chip),
        )

    def to_quad(self, src, slot, kind, q):
        self.copy(src, slot, kind, slot, 4 * self.here.z + q).start()

    def start(self, src):
        here = self.here
        self.to_quad(src, here.chip, 1, here.qx)
        self.to_quad(src, here.chip, 2, here.qy)

        def line(i):
            to = 4 * ((here.z + i) % here.lines) + here.q
            self.copy(src, here.chip, 0, i, to).start()

        loop(1, here.lines, line)

    def wait(self, slot):
        here = self.here
        self.copy(self.buf.at[slot], slot, 0, 0, 4 * here.z + here.qx).wait_recv()

    def column(self, i, process):
        here = self.here
        slot = 4 * here.back_z(i) + here.q
        self.wait(slot)
        self.to_quad(self.buf.at[slot], slot, 1, here.qx)
        self.to_quad(self.buf.at[slot], slot, 2, here.qy)
        process(slot)

    def sides(self, i, process):
        here = self.here
        z = here.back_z(i)
        for q, parity, kind, to in ((here.qx, 0, 2, here.qy), (here.qy, 1, 1, here.qx)):
            slot = 4 * z + q
            self.wait(slot)

            @pl.when(z % 2 == parity)
            def _():
                self.to_quad(self.buf.at[slot], slot, kind, to)

            process(slot)

    def forward(self, process):
        here = self.here

        def both(i):
            self.column(i, process)
            self.sides(i - 1, process)

        loop(1, here.lines, both)
        self.sides(here.lines - 1, process)

    def diagonal(self, i):
        slot = 4 * self.here.back_z(i) + self.here.qd
        self.wait(slot)
        return slot

    def finish(self):
        here = self.here

        def sent(kind, index):
            self.copy(self.buf.at[0], 0, kind, index, 4 * here.z + here.qx).wait_send()

        loop(1, here.lines, lambda i: sent(0, i))

        def rest(z):
            for kind in (1, 2):
                sent(kind, 4 * z + here.q)

            @pl.when(z % 2 == 0)
            def _():
                sent(2, 4 * z + here.qx)

            @pl.when(z % 2 == 1)
            def _():
                sent(1, 4 * z + here.qy)

        loop(0, here.lines, rest)


def project(here, rows, own_rows, weight, outs, out_send):
    outs.buf[here.chip] = dot(own_rows[...], weight[...]).astype(BF16)

    def process(slot):
        out_send[slot] = dot(rows.buf[slot], weight[...]).astype(BF16)
        outs.send(out_send.at[slot], slot)

    rows.forward(process)
    loop(0, here.lines, lambda i: process(rows.diagonal(i)))
    outs.others(outs.wait)
    return jnp.concatenate([outs.buf[i] for i in range(here.n)], axis=1)


def attend(lens, bias, tri, queries, keys, values, q_seq, o_seq):
    seqs, span, width = keys.shape
    pairs = q_seq.shape[1]
    for j in range(pairs):
        q_seq[:, j, :] = queries[:, j * LANES:(j + 1) * LANES].astype(F32)
    low = lax.broadcasted_iota(jnp.int32, (pairs, LANES), 1) < HD
    front = lax.broadcasted_iota(jnp.int32, (pairs, LANES), 0) < pairs // 2
    used = low == front
    heads = 2 * pairs
    count = span // LANES
    pos = lax.broadcasted_iota(jnp.int32, (heads, span), 1)

    def one(s):
        a = q_seq[s]
        r = pltpu.roll(a, HD, 1)
        even = jnp.where(used, jnp.where(front, a, r), 0.0)
        odd = jnp.where(used, jnp.where(front, r, a), 0.0)
        q = jnp.concatenate([even, odd], axis=0).astype(BF16)
        z = lax.dot_general(q, keys[s], (((1,), (1,)), ((), ())), preferred_element_type=F32)
        z = z * HD ** (-0.5) + bias[...]
        valid = pos < lens[s]
        soft = jnp.log(1.0 + jnp.exp(-jnp.abs(z)))
        log_beta = jnp.minimum(z, 0.0) - soft
        log_keep = jnp.where(valid, -jnp.maximum(z, 0.0) - soft, 0.0)
        high = log_keep.astype(BF16)
        rest = (log_keep - high.astype(F32)).astype(BF16)
        parts = [p[:, b * LANES:(b + 1) * LANES] for p in (high, rest) for b in range(count)]
        sums = dot(jnp.concatenate(parts, axis=0), tri[...])
        carry = jnp.zeros((heads, LANES), F32)
        after = [None] * count
        for b in reversed(range(count)):
            here = sums[b * heads:(b + 1) * heads] + sums[(count + b) * heads:(count + b + 1) * heads]
            after[b] = here[:, :LANES] + carry
            carry = carry + here[:, LANES:]
        stick = jnp.where(valid, jnp.exp(log_beta + jnp.concatenate(after, axis=1)), 0.0)
        out = dot(stick.astype(BF16), values[s])
        even, odd = out[:pairs], out[pairs:]
        even_r, odd_r = pltpu.roll(even, HD, 1), pltpu.roll(odd, HD, 1)
        o_seq[s] = jnp.where(
            low, jnp.where(front, even, even_r), jnp.where(front, odd_r, odd)
        )

    many = 4 if seqs % 4 == 0 else 1

    def some(i):
        for j in range(many):
            one(many * i + j)

    loop(0, seqs // many, some)
    return jnp.concatenate([o_seq[:, j, :] for j in range(pairs)], axis=1).astype(BF16)


def layer_kernel(
    n,
    lens, tok, g0, g1, g2, g3, bias_row, routes, route_weights, wq, wk, wv, wo, ck, cv, eg, eu, ed, sg, su, sd,
    joined,
    normed, rows_a, att, rows_b, ffn_in, rows_c, pair_q, pair_o, weight_q, weight_o,
    kw, vw, keys, values, tri, q_seq, o_seq,
    q_buf, q_out, o_buf, o_out, resid1, wts, wts_all, bias,
    gate, up, down, sgate, sup, sdown, total, ysend, quad_buf, line_send, line_buf,
    as_, ar, bs, br, cs, cr, qs, qr, os_, or_, ts, tr, ws, wr, us, ur, vs, vr, ls,
):
    here = Place(n)
    chip, core, partner = here.chip, here.core, here.partner
    seqs = tok.shape[0]
    ff = eg.shape[2]
    own = wq.shape[0]
    barrier = pltpu.get_barrier_semaphore()

    def hello(i):
        pl.semaphore_signal(barrier, inc=1, device_id=(here.device((chip + i) % n),))

    loop(1, n, hello)
    pl.semaphore_signal(barrier, inc=1, device_id=(partner,))
    mine = pl.ds(core * ff, ff)
    cols = pl.ds(core * own, own)
    local = [
        pltpu.make_async_copy(src, dst, ls.at[i])
        for i, (src, dst) in enumerate([
            (wq, pair_q.at[cols]), (wk, kw), (wv, vw), (ck, keys), (cv, values),
            (wo, pair_o.at[cols]),
            (eg.at[0], gate.at[core]), (eu.at[0], up.at[core]), (ed.at[0], down.at[mine]),
            (sg, sgate), (su, sup), (sd, sdown),
        ])
    ]
    for copy in local:
        copy.start()
    normed[...] = rms_scale(tok[...].astype(F32), g0[...]).astype(BF16)
    after = lax.broadcasted_iota(jnp.int32, (LANES, 2 * LANES), 0) > lax.broadcasted_iota(
        jnp.int32, (LANES, 2 * LANES), 1
    )
    every = lax.broadcasted_iota(jnp.int32, (LANES, 2 * LANES), 1) >= LANES
    tri[...] = jnp.where(after | every, 1.0, 0.0).astype(BF16)
    heads = bias.shape[0]
    row = lax.broadcasted_iota(jnp.int32, (heads, heads), 0)
    head = jnp.where(row < heads // 2, 2 * row, 2 * row - heads + 1)
    at_head = lax.broadcasted_iota(jnp.int32, (heads, heads), 1) == head
    bias[...] = jnp.sum(jnp.where(at_head, bias_row[...], 0.0), axis=1, keepdims=True)
    expert = lax.broadcasted_iota(jnp.int32, (2 * n, seqs), 0)
    dense = jnp.zeros((2 * n, seqs), F32)
    for k in range(routes.shape[0]):
        dense = dense + jnp.where(
            routes[k:k + 1, :] == expert, route_weights[k:k + 1, :], 0.0
        )
    wts[...] = jnp.zeros_like(wts)
    for c in range(n):
        wts[c, :, :seqs] = dense[2 * c:2 * c + 2]
    pl.semaphore_wait(barrier, n)

    first = Gather(here, rows_a, as_, ar)
    second = Gather(here, rows_b, bs, br)
    third = Gather(here, rows_c, cs, cr)
    q_outs = Direct(here, q_buf, qs, qr)
    o_outs = Direct(here, o_buf, os_, or_)
    tabs = Direct(here, wts_all, ts, tr)
    swaps = [
        remote(src, dst, ws.at[i], wr.at[i], partner)
        for i, (src, dst) in enumerate([
            (wq, pair_q.at[cols]), (wo, pair_o.at[cols]),
            (eg.at[0], gate.at[core]), (eu.at[0], up.at[core]), (ed.at[0], down.at[mine]),
        ])
    ]
    first.start(normed)
    for copy in swaps:
        copy.start()
    tabs.others(lambda c: tabs.send(wts.at[c], c))
    wts_all[chip] = wts[chip]
    for copy in local[:3]:
        copy.wait()
    wide, width = tok.shape[1], wk.shape[1]
    joined[:, wide:wide + width] = dot(normed[...], kw[...]).astype(BF16)
    joined[:, wide + width:] = dot(normed[...], vw[...]).astype(BF16)
    swaps[0].wait_recv()
    weight_q[...] = pair_q[...].T
    queries = project(here, first, normed, weight_q, q_outs, q_out)
    for copy in local[3:]:
        copy.wait()
    att[...] = attend(lens, bias, tri, queries, keys, values, q_seq, o_seq)

    second.start(att)
    swaps[1].wait_recv()
    weight_o[...] = pair_o[...].T
    mixed = project(here, second, att, weight_o, o_outs, o_out)
    resid1[...] = tok[...].astype(F32) + rms_scale(mixed.astype(F32), g1[...])
    ffn_in[...] = rms_scale(resid1[...], g2[...]).astype(BF16)

    third.start(ffn_in)
    rows_c[chip] = ffn_in[...]
    tabs.others(tabs.wait)
    for copy in swaps[2:]:
        copy.wait_recv()
    third.forward(lambda slot: None)
    per = Z_PER_GROUP if here.lines % Z_PER_GROUP == 0 else 1
    eye = (
        lax.broadcasted_iota(jnp.int32, (seqs, wts.shape[2]), 0)
        == lax.broadcasted_iota(jnp.int32, (seqs, wts.shape[2]), 1)
    )
    peers = (here.qx, here.qy, here.qd)

    def quad_copy(p, z):
        return remote(
            ysend.at[4 * z + peers[p]], quad_buf.at[p, z], us.at[p, z], ur.at[p, z],
            here.device(4 * here.z + peers[p]),
        )

    def line_copy(i, slot, z):
        return remote(
            line_send.at[i], line_buf.at[slot], vs.at[i], vr.at[slot],
            here.device(4 * z + here.q),
        )

    def group(g):
        slots = []
        for j in range(per):
            i = g * per + j
            third.diagonal(i)
            slots += [4 * here.back_z(i) + q for q in range(4)]
        x = jnp.concatenate([rows_c[slot] for slot in slots], axis=0)
        halves = []
        for e in range(2):
            columns = []
            for slot in slots:
                row = wts_all[slot][e:e + 1]
                columns.append(jnp.sum(jnp.where(eye, row, 0.0), axis=1, keepdims=True))
            scale = jnp.concatenate(columns, axis=0)
            hidden = jax.nn.silu(dot(x, gate[e])) * dot(x, up[e])
            halves.append((hidden * scale).astype(BF16))
        y = dot(jnp.concatenate(halves, axis=1), down[...]).astype(BF16)
        for j, slot in enumerate(slots):
            ysend[slot] = y[j * seqs:(j + 1) * seqs]
        for j in range(per):
            for p in (2, 0, 1):
                quad_copy(p, here.back_z(g * per + j)).start()

    def quad_sum(i):
        z = here.back_z(i)
        acc = ysend[4 * z + here.q].astype(F32)
        for p in range(3):
            quad_copy(p, z).wait_recv()
            acc = acc + quad_buf[p, z].astype(F32)
        return z, acc

    def pass_on(i):
        z, acc = quad_sum(i)
        line_send[i] = acc.astype(BF16)
        line_copy(i, here.z, z).start()

    groups = here.lines // per
    group(0)

    def later(g):
        group(g)
        for j in range(per):
            i = (g - 1) * per + j

            @pl.when(i > 0)
            def _():
                pass_on(i)

    loop(1, groups, later)
    mid = (jax.nn.silu(dot(ffn_in[...], sgate[...])) * dot(ffn_in[...], sup[...])).astype(BF16)
    total[...] = dot(mid, sdown[...])
    loop(max((groups - 1) * per, 1), here.lines, pass_on)
    _, acc = quad_sum(0)
    total[...] += acc

    def add(i):
        z = (here.z + i) % here.lines
        line_copy(0, z, here.z).wait_recv()
        total[...] += line_buf[z].astype(F32)

    loop(1, here.lines, add)
    joined[:, :wide] = (resid1[...] + rms_scale(total[...], g3[...])).astype(BF16)

    for copy in swaps:
        copy.wait_send()
    for plane in (first, second, third):
        plane.finish()
    for plane in (q_outs, o_outs, tabs):
        plane.others(plane.wait_sent)

    def sent(z):
        for p in range(3):
            quad_copy(p, z).wait_send()

    loop(0, here.lines, sent)
    loop(1, here.lines, lambda i: line_copy(i, 0, here.z).wait_send())


def split_kernel(joined, layer_out, new_keys, new_values):
    wide, keys = layer_out.shape[1], new_keys.shape[1]
    layer_out[...] = joined[:, :wide]
    new_keys[...] = joined[:, wide:wide + keys]
    new_values[...] = joined[:, wide + keys:]


def run_layer(n, lens, tokens, gains, bias, routes, route_weights, wq, wk, wv, wo, ck, cv, eg, eu, ed, sg, su, sd):
    vm = pl.BlockSpec(memory_space=pltpu.VMEM)
    hbm = pl.BlockSpec(memory_space=pl.ANY)
    seqs, wide = tokens.shape
    own = wq.shape[0]
    ff = eg.shape[2]
    lines = n // 4
    pairs = n * 2 * own // LANES
    sems = pltpu.SemaphoreType.DMA
    half = lambda *shape: pltpu.VMEM(shape, BF16)
    full = lambda *shape: pltpu.VMEM(shape, F32)
    joined = pl.pallas_call(
        functools.partial(layer_kernel, n),
        out_shape=jax.ShapeDtypeStruct((seqs, wide + wk.shape[1] + wv.shape[1]), BF16),
        in_specs=[pl.BlockSpec(memory_space=pltpu.SMEM)] + [vm] * 8 + [hbm] * 12,
        out_specs=vm,
        scratch_shapes=[
            half(seqs, wide), half(n, seqs, wide), half(seqs, wide), half(n, seqs, wide),
            half(seqs, wide), half(n, seqs, wide),
            half(2 * own, wide), half(2 * own, wide), half(wide, 2 * own), half(wide, 2 * own),
            half(*wk.shape), half(*wv.shape), half(*ck.shape), half(*cv.shape),
            half(LANES, 2 * LANES), full(seqs, pairs, LANES), full(seqs, pairs, LANES),
            half(n, seqs, 2 * own), half(n, seqs, 2 * own),
            half(n, seqs, 2 * own), half(n, seqs, 2 * own),
            full(seqs, wide), full(n, 2, LANES), full(n, 2, LANES), full(bias.shape[1], 1),
            half(2, wide, ff), half(2, wide, ff), half(2 * ff, wide),
            half(*sg.shape), half(*su.shape), half(*sd.shape),
            full(seqs, wide), half(n, seqs, wide), half(3, lines, seqs, wide),
            half(lines, seqs, wide), half(lines, seqs, wide),
            sems((3, n)), sems((n,)), sems((3, n)), sems((n,)), sems((3, n)), sems((n,)),
            sems((n,)), sems((n,)), sems((n,)), sems((n,)), sems((n,)), sems((n,)),
            sems((5,)), sems((5,)), sems((3, lines)), sems((3, lines)),
            sems((lines,)), sems((lines,)), sems((12,)),
        ],
        compiler_params=pltpu.CompilerParams(
            collective_id=0, has_side_effects=True, vmem_limit_bytes=62 << 20
        ),
    )(lens, tokens, *gains, bias, routes, route_weights, wq, wk, wv, wo, ck, cv, eg, eu, ed, sg, su, sd)
    return pl.pallas_call(
        split_kernel,
        out_shape=(
            jax.ShapeDtypeStruct((seqs, wide), BF16),
            jax.ShapeDtypeStruct((seqs, wk.shape[1]), BF16),
            jax.ShapeDtypeStruct((seqs, wv.shape[1]), BF16),
        ),
        in_specs=[vm],
        out_specs=(vm,) * 3,
    )(joined)


def body(
    tokens,
    lengths,
    cache_keys,
    cache_values,
    mix_gain,
    mix_out_gain,
    ffn_gain,
    ffn_out_gain,
    query_weight,
    key_weight,
    value_weight,
    head_bias,
    output_weight,
    routes,
    route_weights,
    expert_gate,
    expert_up,
    expert_down,
    shared_gate,
    shared_up,
    shared_down,
):
    n = lax.axis_size("ep") // 2
    gains = [g[None] for g in (mix_gain, mix_out_gain, ffn_gain, ffn_out_gain)]
    return run_layer(
        n, lengths, tokens, gains, head_bias[None], routes.T, route_weights.T, query_weight.T, key_weight, value_weight,
        output_weight.T, cache_keys, cache_values,
        expert_gate, expert_up, expert_down, shared_gate, shared_up, shared_down,
    )


def solution(mesh):
    in_specs = (
        P("ep", None),
        P("ep"),
        P("ep", None, None),
        P("ep", None, None),
        P(),
        P(),
        P(),
        P(),
        P(None, "ep"),
        P(),
        P(),
        P(),
        P(None, "ep"),
        P("ep", None),
        P("ep", None),
        P("ep", None, None),
        P("ep", None, None),
        P("ep", None, None),
        P(),
        P(),
        P(),
    )
    out_specs = (P("ep", None), P("ep", None), P("ep", None))
    return jax.shard_map(body, mesh=mesh, in_specs=in_specs, out_specs=out_specs, check_vma=False)
```

profile of v0, /device:TPU:0, one launch (start us, length us, event | category | flops | bytes accessed | tf_op | source)
XLA Modules:
  0.0 91.4 jit_solution(9551666887246769456)
XLA Ops:
  0.6 89.2 %shard_map.220.joined = bf16[16,2304]{1,0:T(8,128)(2,1)} custom-call(s32[16]{0:T(128)} %lens.1, bf16[16,2048]{1,0:T(8,128)(2,1)} %tok.1, f32[1,2048]{1,0:T(1,128)} %bitcast.11, f32[1,2048]{1,0:T(1,128)} %bitcast.12, f32[1,2048]{1,0:T(1,128)} %bitcast.13, f32[1,2048]{1,0:T(1,128)} %bitcast.14, f32[1,32]{1,0:T(1,128)} %bitcast.17, s32[6,16]{1,0:T(8,128)} %bitcast.15, ...), custom_call_target="tpu_custom_call" | custom-call | tf_op jit(solution)/shard_map/pallas_call | solution.py:457
  89.9 1.5 %shard_map.221 = (bf16[16,2048]{1,0:T(8,128)(2,1)}, bf16[16,128]{1,0:T(8,128)(2,1)}, bf16[16,128]{1,0:T(8,128)(2,1)}) custom-call(bf16[16,2304]{1,0:T(8,128)(2,1)} %shard_map.220.joined), custom_call_target="tpu_custom_call" | custom-call | tf_op jit(solution)/shard_map/pallas_call | solution.py:484
where the time goes:
time: 91.6 us; the launch traced here: 91.4 us
  Pallas kernels  90.7 us (99%)
    pallas_call x1, Pallas kernels, run_layer(): pl.pallas_call(functools.partial(layer_kernel, n), out_shape=jax.ShapeDty...  89.2 us

commit v1 on v0

--- a/solution.py
+++ b/solution.py
@@ -11,7 +11,6 @@
 LANES = 128
 F32 = jnp.float32
 BF16 = jnp.bfloat16
-Z_PER_GROUP = 2
 
 
 def rms_scale(rows, gain):
@@ -243,11 +242,11 @@
     n,
     lens, tok, g0, g1, g2, g3, bias_row, routes, route_weights, wq, wk, wv, wo, ck, cv, eg, eu, ed, sg, su, sd,
     joined,
-    normed, rows_a, att, rows_b, ffn_in, rows_c, pair_q, pair_o, weight_q, weight_o,
+    normed, rows_a, att, rows_b, ffn_in, rows_c, pair_q, weight_q, line_o,
     kw, vw, keys, values, tri, q_seq, o_seq,
     q_buf, q_out, o_buf, o_out, resid1, wts, wts_all, bias,
     gate, up, down, sgate, sup, sdown, total, ysend, quad_buf, line_send, line_buf,
-    as_, ar, bs, br, cs, cr, qs, qr, os_, or_, ts, tr, ws, wr, us, ur, vs, vr, ls,
+    as_, ar, bs, br, cs, cr, qs, qr, os_, or_, ts, tr, ws, wr, us, ur, vs, vr, xs, xr, fs, fr, ls,
 ):
     here = Place(n)
     chip, core, partner = here.chip, here.core, here.partner
@@ -267,7 +266,7 @@
         pltpu.make_async_copy(src, dst, ls.at[i])
         for i, (src, dst) in enumerate([
             (wq, pair_q.at[cols]), (wk, kw), (wv, vw), (ck, keys), (cv, values),
-            (wo, pair_o.at[cols]),
+            (wo, line_o.at[here.z, cols]),
             (eg.at[0], gate.at[core]), (eu.at[0], up.at[core]), (ed.at[0], down.at[mine]),
             (sg, sgate), (su, sup), (sd, sdown),
         ])
@@ -297,20 +296,40 @@
     pl.semaphore_wait(barrier, n)
 
     first = Gather(here, rows_a, as_, ar)
-    second = Gather(here, rows_b, bs, br)
     third = Gather(here, rows_c, cs, cr)
     q_outs = Direct(here, q_buf, qs, qr)
-    o_outs = Direct(here, o_buf, os_, or_)
     tabs = Direct(here, wts_all, ts, tr)
     swaps = [
         remote(src, dst, ws.at[i], wr.at[i], partner)
         for i, (src, dst) in enumerate([
-            (wq, pair_q.at[cols]), (wo, pair_o.at[cols]),
+            (wq, pair_q.at[cols]),
             (eg.at[0], gate.at[core]), (eu.at[0], up.at[core]), (ed.at[0], down.at[mine]),
         ])
     ]
+    peers = (here.qx, here.qy, here.qd)
+
+    def line_weight(src, slot, i, to):
+        return remote(src, line_o.at[slot, cols], xs.at[i], xr.at[slot], here.device(4 * to + here.q))
+
+    def pair_weight(src, slot):
+        return remote(src, line_o.at[slot, cols], fs.at[slot], fr.at[slot], partner)
+
+    def quad_rows(p):
+        return remote(
+            att, rows_b.at[here.q], bs.at[p], br.at[here.q], here.device(4 * here.z + peers[p])
+        )
+
+    def quad_outs(p):
+        return remote(
+            o_out.at[peers[p]], o_buf.at[here.q], os_.at[p], or_.at[here.q],
+            here.device(4 * here.z + peers[p]),
+        )
+
     first.start(normed)
-    for copy in swaps:
+    swaps[0].start()
+    loop(1, here.lines, lambda i: line_weight(wo, here.z, i, (here.z + i) % here.lines).start())
+    pair_weight(wo, here.z).start()
+    for copy in swaps[1:]:
         copy.start()
     tabs.others(lambda c: tabs.send(wts.at[c], c))
     wts_all[chip] = wts[chip]
@@ -326,25 +345,51 @@
         copy.wait()
     att[...] = attend(lens, bias, tri, queries, keys, values, q_seq, o_seq)
 
-    second.start(att)
-    swaps[1].wait_recv()
-    weight_o[...] = pair_o[...].T
-    mixed = project(here, second, att, weight_o, o_outs, o_out)
+    for p in (2, 0, 1):
+        quad_rows(p).start()
+
+    def forward_weight(i):
+        slot = here.back_z(i)
+        line_weight(wo, slot, 0, here.z).wait_recv()
+        pair_weight(line_o.at[slot, cols], slot).start()
+
+    loop(1, here.lines, forward_weight)
+    rows_b[here.q] = att[...]
+    loop(0, here.lines, lambda z: pair_weight(wo, z).wait_recv())
+    for p in range(3):
+        remote(
+            att, rows_b.at[peers[p]], bs.at[p], br.at[peers[p]], partner
+        ).wait_recv()
+    part = lax.dot_general(
+        rows_b[...].reshape(4 * seqs, -1), line_o[...].reshape(2 * own * here.lines, -1),
+        (((1,), (1,)), ((), ())), preferred_element_type=F32,
+    ).astype(BF16)
+    for q in range(4):
+        o_out[q] = part[q * seqs:(q + 1) * seqs]
+    for p in (2, 0, 1):
+        quad_outs(p).start()
+    o_buf[here.q] = o_out[here.q]
+    for p in range(3):
+        remote(
+            o_out.at[0], o_buf.at[peers[p]], os_.at[p], or_.at[peers[p]], partner
+        ).wait_recv()
+    mixed = jnp.concatenate([
+        o_buf[q, :, 2 * own * z:2 * own * (z + 1)] for z in range(here.lines) for q in range(4)
+    ], axis=1)
     resid1[...] = tok[...].astype(F32) + rms_scale(mixed.astype(F32), g1[...])
     ffn_in[...] = rms_scale(resid1[...], g2[...]).astype(BF16)
 
     third.start(ffn_in)
     rows_c[chip] = ffn_in[...]
+    mid = (jax.nn.silu(dot(ffn_in[...], sgate[...])) * dot(ffn_in[...], sup[...])).astype(BF16)
+    total[...] = dot(mid, sdown[...])
     tabs.others(tabs.wait)
-    for copy in swaps[2:]:
+    for copy in swaps[1:]:
         copy.wait_recv()
-    third.forward(lambda slot: None)
-    per = Z_PER_GROUP if here.lines % Z_PER_GROUP == 0 else 1
     eye = (
         lax.broadcasted_iota(jnp.int32, (seqs, wts.shape[2]), 0)
         == lax.broadcasted_iota(jnp.int32, (seqs, wts.shape[2]), 1)
     )
-    peers = (here.qx, here.qy, here.qd)
 
     def quad_copy(p, z):
         return remote(
@@ -358,12 +403,8 @@
             here.device(4 * z + here.q),
         )
 
-    def group(g):
-        slots = []
-        for j in range(per):
-            i = g * per + j
-            third.diagonal(i)
-            slots += [4 * here.back_z(i) + q for q in range(4)]
+    def group(i):
+        slots = [4 * here.back_z(i) + q for q in range(4)]
         x = jnp.concatenate([rows_c[slot] for slot in slots], axis=0)
         halves = []
         for e in range(2):
@@ -377,9 +418,8 @@
         y = dot(jnp.concatenate(halves, axis=1), down[...]).astype(BF16)
         for j, slot in enumerate(slots):
             ysend[slot] = y[j * seqs:(j + 1) * seqs]
-        for j in range(per):
-            for p in (2, 0, 1):
-                quad_copy(p, here.back_z(g * per + j)).start()
+        for p in (2, 0, 1):
+            quad_copy(p, here.back_z(i)).start()
 
     def quad_sum(i):
         z = here.back_z(i)
@@ -394,22 +434,22 @@
         line_send[i] = acc.astype(BF16)
         line_copy(i, here.z, z).start()
 
-    groups = here.lines // per
-    group(0)
-
-    def later(g):
-        group(g)
-        for j in range(per):
-            i = (g - 1) * per + j
-
-            @pl.when(i > 0)
-            def _():
-                pass_on(i)
-
-    loop(1, groups, later)
-    mid = (jax.nn.silu(dot(ffn_in[...], sgate[...])) * dot(ffn_in[...], sup[...])).astype(BF16)
-    total[...] = dot(mid, sdown[...])
-    loop(max((groups - 1) * per, 1), here.lines, pass_on)
+    def stage(i):
+        third.sides(i, lambda slot: None)
+
+        @pl.when(i + 1 < here.lines)
+        def _():
+            third.column(i + 1, lambda slot: None)
+
+        third.diagonal(i)
+        group(i)
+
+        @pl.when(i > 1)
+        def _():
+            pass_on(i - 1)
+
+    loop(0, here.lines, stage)
+    loop(max(here.lines - 1, 1), here.lines, pass_on)
     _, acc = quad_sum(0)
     total[...] += acc
 
@@ -423,9 +463,9 @@
 
     for copy in swaps:
         copy.wait_send()
-    for plane in (first, second, third):
+    for plane in (first, third):
         plane.finish()
-    for plane in (q_outs, o_outs, tabs):
+    for plane in (q_outs, tabs):
         plane.others(plane.wait_sent)
 
     def sent(z):
@@ -433,6 +473,11 @@
             quad_copy(p, z).wait_send()
 
     loop(0, here.lines, sent)
+    loop(1, here.lines, lambda i: line_weight(wo, here.z, i, here.z).wait_send())
+    loop(0, here.lines, lambda z: pair_weight(wo, z).wait_send())
+    for p in range(3):
+        quad_rows(p).wait_send()
+        quad_outs(p).wait_send()
     loop(1, here.lines, lambda i: line_copy(i, 0, here.z).wait_send())
 
 
@@ -460,21 +505,22 @@
         in_specs=[pl.BlockSpec(memory_space=pltpu.SMEM)] + [vm] * 8 + [hbm] * 12,
         out_specs=vm,
         scratch_shapes=[
-            half(seqs, wide), half(n, seqs, wide), half(seqs, wide), half(n, seqs, wide),
+            half(seqs, wide), half(n, seqs, wide), half(seqs, wide), half(4, seqs, wide),
             half(seqs, wide), half(n, seqs, wide),
-            half(2 * own, wide), half(2 * own, wide), half(wide, 2 * own), half(wide, 2 * own),
+            half(2 * own, wide), half(wide, 2 * own), half(lines, 2 * own, wide),
             half(*wk.shape), half(*wv.shape), half(*ck.shape), half(*cv.shape),
             half(LANES, 2 * LANES), full(seqs, pairs, LANES), full(seqs, pairs, LANES),
             half(n, seqs, 2 * own), half(n, seqs, 2 * own),
-            half(n, seqs, 2 * own), half(n, seqs, 2 * own),
+            half(4, seqs, 2 * own * lines), half(4, seqs, 2 * own * lines),
             full(seqs, wide), full(n, 2, LANES), full(n, 2, LANES), full(bias.shape[1], 1),
             half(2, wide, ff), half(2, wide, ff), half(2 * ff, wide),
             half(*sg.shape), half(*su.shape), half(*sd.shape),
             full(seqs, wide), half(n, seqs, wide), half(3, lines, seqs, wide),
             half(lines, seqs, wide), half(lines, seqs, wide),
-            sems((3, n)), sems((n,)), sems((3, n)), sems((n,)), sems((3, n)), sems((n,)),
-            sems((n,)), sems((n,)), sems((n,)), sems((n,)), sems((n,)), sems((n,)),
-            sems((5,)), sems((5,)), sems((3, lines)), sems((3, lines)),
+            sems((3, n)), sems((n,)), sems((3,)), sems((4,)), sems((3, n)), sems((n,)),
+            sems((n,)), sems((n,)), sems((3,)), sems((4,)), sems((n,)), sems((n,)),
+            sems((4,)), sems((4,)), sems((3, lines)), sems((3, lines)),
+            sems((lines,)), sems((lines,)), sems((lines,)), sems((lines,)),
             sems((lines,)), sems((lines,)), sems((12,)),
         ],
         compiler_params=pltpu.CompilerParams(

time: 91.6 us -> 107 us (1.17)
  Pallas kernels: 90.7 us -> 106 us
    pallas_call x1, Pallas kernels: 89.2 us -> 104 us  [run_layer(): pl.pallas_call(functools.partial(layer_kernel, n), out_shape=jax.ShapeDty...]
where the time goes in v1:
time: 107 us
  Pallas kernels  106 us (99%)
    pallas_call x1, Pallas kernels, run_layer(): pl.pallas_call(functools.partial(layer_kernel, n), out_shape=jax.ShapeDty...  104 us

profile of v1, /device:TPU:0, one launch (start us, length us, event | category | flops | bytes accessed | tf_op | source)
XLA Modules:
  0.0 106.5 jit_solution(5378070631752092431)
XLA Ops:
  0.6 104.3 %shard_map.220.joined = bf16[16,2304]{1,0:T(8,128)(2,1)} custom-call(s32[16]{0:T(128)} %lens.1, bf16[16,2048]{1,0:T(8,128)(2,1)} %tok.1, f32[1,2048]{1,0:T(1,128)} %bitcast.11, f32[1,2048]{1,0:T(1,128)} %bitcast.12, f32[1,2048]{1,0:T(1,128)} %bitcast.13, f32[1,2048]{1,0:T(1,128)} %bitcast.14, f32[1,32]{1,0:T(1,128)} %bitcast.17, s32[6,16]{1,0:T(8,128)} %bitcast.15, ...), custom_call_target="tpu_custom_call" | custom-call | tf_op jit(solution)/shard_map/pallas_call | solution.py:502
  105.0 1.5 %shard_map.221 = (bf16[16,2048]{1,0:T(8,128)(2,1)}, bf16[16,128]{1,0:T(8,128)(2,1)}, bf16[16,128]{1,0:T(8,128)(2,1)}) custom-call(bf16[16,2304]{1,0:T(8,128)(2,1)} %shard_map.220.joined), custom_call_target="tpu_custom_call" | custom-call | tf_op jit(solution)/shard_map/pallas_call | solution.py:530

commit v2 on v0

--- a/solution.py
+++ b/solution.py
@@ -82,6 +82,10 @@
             self.recv_sems.at[chip], self.here.partner,
         ).wait_send()
 
+    def gathered(self):
+        self.others(self.wait)
+        return jnp.concatenate([self.buf[i] for i in range(self.here.n)], axis=1)
+
     def others(self, one):
         here = self.here
         loop(1, here.n, lambda i: one((here.chip + i) % here.n))
@@ -181,13 +185,13 @@
         out_send[slot] = dot(rows.buf[slot], weight[...]).astype(BF16)
         outs.send(out_send.at[slot], slot)
 
-    rows.forward(process)
-    loop(0, here.lines, lambda i: process(rows.diagonal(i)))
-    outs.others(outs.wait)
-    return jnp.concatenate([outs.buf[i] for i in range(here.n)], axis=1)
-
-
-def attend(lens, bias, tri, queries, keys, values, q_seq, o_seq):
+    with jax.named_scope("qfwd"):
+        rows.forward(process)
+    with jax.named_scope("qdiag"):
+        loop(0, here.lines, lambda i: process(rows.diagonal(i)))
+
+
+def attend(lens, bias, tri, queries, keys, values, q_seq, o_seq, att, send_half, pass_weights):
     seqs, span, width = keys.shape
     pairs = q_seq.shape[1]
     for j in range(pairs):
@@ -235,19 +239,38 @@
         for j in range(many):
             one(many * i + j)
 
-    loop(0, seqs // many, some)
-    return jnp.concatenate([o_seq[:, j, :] for j in range(pairs)], axis=1).astype(BF16)
+    steps = seqs // many
+    mid, late = steps // 2, max(steps // 2, steps - 1)
+
+    def finish(h):
+        rows = pl.ds(h * (seqs // 2), seqs // 2)
+        att[rows] = jnp.concatenate([o_seq[rows, j, :] for j in range(pairs)], axis=1).astype(BF16)
+        send_half(h)
+
+    def stage(i):
+        @pl.when(i == late)
+        def _():
+            pass_weights()
+
+        some(i)
+
+        @pl.when(i == mid - 1)
+        def _():
+            finish(0)
+
+    loop(0, steps, stage)
+    finish(1)
 
 
 def layer_kernel(
     n,
     lens, tok, g0, g1, g2, g3, bias_row, routes, route_weights, wq, wk, wv, wo, ck, cv, eg, eu, ed, sg, su, sd,
     joined,
-    normed, rows_a, att, rows_b, ffn_in, rows_c, pair_q, pair_o, weight_q, weight_o,
+    normed, rows_a, att, rows_b, ffn_in, rows_c, pair_q, weight_q, quad_o,
     kw, vw, keys, values, tri, q_seq, o_seq,
     q_buf, q_out, o_buf, o_out, resid1, wts, wts_all, bias,
     gate, up, down, sgate, sup, sdown, total, ysend, quad_buf, line_send, line_buf,
-    as_, ar, bs, br, cs, cr, qs, qr, os_, or_, ts, tr, ws, wr, us, ur, vs, vr, ls,
+    as_, ar, bs, br, cs, cr, qs, qr, os_, or_, ts, tr, ws, wr, us, ur, vs, vr, xs, xr, ys, yr, fs, fr, ls,
 ):
     here = Place(n)
     chip, core, partner = here.chip, here.core, here.partner
@@ -267,7 +290,7 @@
         pltpu.make_async_copy(src, dst, ls.at[i])
         for i, (src, dst) in enumerate([
             (wq, pair_q.at[cols]), (wk, kw), (wv, vw), (ck, keys), (cv, values),
-            (wo, pair_o.at[cols]),
+            (wo, quad_o.at[here.q, cols]),
             (eg.at[0], gate.at[core]), (eu.at[0], up.at[core]), (ed.at[0], down.at[mine]),
             (sg, sgate), (su, sup), (sd, sdown),
         ])
@@ -294,21 +317,71 @@
     wts[...] = jnp.zeros_like(wts)
     for c in range(n):
         wts[c, :, :seqs] = dense[2 * c:2 * c + 2]
-    pl.semaphore_wait(barrier, n)
+    with jax.named_scope("barrier"):
+        pl.semaphore_wait(barrier, n)
 
     first = Gather(here, rows_a, as_, ar)
-    second = Gather(here, rows_b, bs, br)
     third = Gather(here, rows_c, cs, cr)
     q_outs = Direct(here, q_buf, qs, qr)
-    o_outs = Direct(here, o_buf, os_, or_)
     tabs = Direct(here, wts_all, ts, tr)
     swaps = [
         remote(src, dst, ws.at[i], wr.at[i], partner)
         for i, (src, dst) in enumerate([
-            (wq, pair_q.at[cols]), (wo, pair_o.at[cols]),
+            (wq, pair_q.at[cols]),
             (eg.at[0], gate.at[core]), (eu.at[0], up.at[core]), (ed.at[0], down.at[mine]),
         ])
     ]
+    peers = (here.qx, here.qy, here.qd)
+    cut = own // 2
+    part_of = seqs // 2
+
+    def quad_weight(p):
+        mine_o = quad_o.at[here.q, cols]
+        return remote(mine_o, mine_o, xs.at[p], xr.at[p], here.device(4 * here.z + peers[p]))
+
+    def quad_weight_in(p):
+        there = quad_o.at[peers[p], cols]
+        return remote(there, there, xs.at[p], xr.at[p], partner)
+
+    def relay_weight(p):
+        half_o = quad_o.at[peers[p], pl.ds(core * own + p * cut, cut)]
+        return remote(half_o, half_o, ys.at[p], yr.at[p], here.device(4 * here.z + peers[1 - p]))
+
+    def relay_weight_in(p):
+        half_o = quad_o.at[here.qd, pl.ds(core * own + p * cut, cut)]
+        return remote(half_o, half_o, ys.at[p], yr.at[p], partner)
+
+    def pair_weight(q):
+        held = quad_o.at[q, cols]
+        return remote(held, held, fs.at[q], fr.at[q], partner)
+
+    def pair_weight_in(q):
+        held = quad_o.at[q, pl.ds((1 - core) * own, own)]
+        return remote(held, held, fs.at[q], fr.at[q], partner)
+
+    def line_rows(i, h):
+        z = (here.z + i) % here.lines
+        some = pl.ds(h * part_of, part_of)
+        return remote(
+            att.at[some], rows_b.at[here.z, some], bs.at[h, i], br.at[h, here.z],
+            here.device(4 * z + here.q),
+        )
+
+    def line_rows_in(i, h):
+        z = here.back_z(i)
+        some = pl.ds(h * part_of, part_of)
+        return remote(att.at[some], rows_b.at[z, some], bs.at[h, i], br.at[h, z], partner)
+
+    def line_outs(i):
+        z = (here.z + i) % here.lines
+        return remote(
+            o_out.at[z], o_buf.at[here.z], os_.at[i], or_.at[here.z], here.device(4 * z + here.q)
+        )
+
+    def line_outs_in(i):
+        z = here.back_z(i)
+        return remote(o_out.at[z], o_buf.at[z], os_.at[i], or_.at[z], partner)
+
     first.start(normed)
     for copy in swaps:
         copy.start()
@@ -321,30 +394,68 @@
     joined[:, wide + width:] = dot(normed[...], vw[...]).astype(BF16)
     swaps[0].wait_recv()
     weight_q[...] = pair_q[...].T
-    queries = project(here, first, normed, weight_q, q_outs, q_out)
+    project(here, first, normed, weight_q, q_outs, q_out)
     for copy in local[3:]:
         copy.wait()
-    att[...] = attend(lens, bias, tri, queries, keys, values, q_seq, o_seq)
-
-    second.start(att)
-    swaps[1].wait_recv()
-    weight_o[...] = pair_o[...].T
-    mixed = project(here, second, att, weight_o, o_outs, o_out)
+    quad_weight(0).start()
+    quad_weight(1).start()
+    pair_weight(here.q).start()
+    with jax.named_scope("qret"):
+        queries = q_outs.gathered()
+
+    def send_half(h):
+        some = pl.ds(h * part_of, part_of)
+        rows_b[here.z, some] = att[some]
+        loop(1, here.lines, lambda i: line_rows(i, h).start())
+
+    def pass_weights():
+        for p in range(2):
+            quad_weight_in(p).wait_recv()
+            relay_weight(p).start()
+        for p in range(2):
+            pair_weight(peers[p]).start()
+
+    with jax.named_scope("attend"):
+        attend(lens, bias, tri, queries, keys, values, q_seq, o_seq, att, send_half, pass_weights)
+
+    with jax.named_scope("weights"):
+        for p in range(2):
+            relay_weight_in(p).wait_recv()
+        pair_weight(here.qd).start()
+        for q in range(4):
+            pair_weight_in(q).wait_recv()
+
+    with jax.named_scope("rows_b"):
+        for h in range(2):
+            loop(1, here.lines, lambda i: line_rows_in(i, h).wait_recv())
+    with jax.named_scope("odot"):
+        part = lax.dot_general(
+            rows_b[...].reshape(here.lines * seqs, -1), quad_o[...].reshape(8 * own, -1),
+            (((1,), (1,)), ((), ())), preferred_element_type=F32,
+        ).astype(BF16)
+        o_out[...] = part.reshape(here.lines, seqs, 8 * own)
+    loop(1, here.lines, lambda i: line_outs(i).start())
+    o_buf[here.z] = o_out[here.z]
+    with jax.named_scope("oret"):
+        loop(1, here.lines, lambda i: line_outs_in(i).wait_recv())
+    mixed = jnp.concatenate([o_buf[z] for z in range(here.lines)], axis=1)
     resid1[...] = tok[...].astype(F32) + rms_scale(mixed.astype(F32), g1[...])
     ffn_in[...] = rms_scale(resid1[...], g2[...]).astype(BF16)
 
     third.start(ffn_in)
     rows_c[chip] = ffn_in[...]
+    mid = (jax.nn.silu(dot(ffn_in[...], sgate[...])) * dot(ffn_in[...], sup[...])).astype(BF16)
+    total[...] = dot(mid, sdown[...])
     tabs.others(tabs.wait)
-    for copy in swaps[2:]:
+    for copy in swaps[1:]:
         copy.wait_recv()
-    third.forward(lambda slot: None)
+    with jax.named_scope("fwd3"):
+        third.forward(lambda slot: None)
     per = Z_PER_GROUP if here.lines % Z_PER_GROUP == 0 else 1
     eye = (
         lax.broadcasted_iota(jnp.int32, (seqs, wts.shape[2]), 0)
         == lax.broadcasted_iota(jnp.int32, (seqs, wts.shape[2]), 1)
     )
-    peers = (here.qx, here.qy, here.qd)
 
     def quad_copy(p, z):
         return remote(
@@ -377,7 +488,7 @@
         y = dot(jnp.concatenate(halves, axis=1), down[...]).astype(BF16)
         for j, slot in enumerate(slots):
             ysend[slot] = y[j * seqs:(j + 1) * seqs]
-        for j in range(per):
+        for j in reversed(range(per)):
             for p in (2, 0, 1):
                 quad_copy(p, here.back_z(g * per + j)).start()
 
@@ -395,21 +506,18 @@
         line_copy(i, here.z, z).start()
 
     groups = here.lines // per
-    group(0)
-
-    def later(g):
+    with jax.named_scope("groupA"):
+        group(groups - 1)
+
+    def later(k):
+        g = groups - 1 - k
         group(g)
-        for j in range(per):
-            i = (g - 1) * per + j
-
-            @pl.when(i > 0)
-            def _():
-                pass_on(i)
-
-    loop(1, groups, later)
-    mid = (jax.nn.silu(dot(ffn_in[...], sgate[...])) * dot(ffn_in[...], sup[...])).astype(BF16)
-    total[...] = dot(mid, sdown[...])
-    loop(max((groups - 1) * per, 1), here.lines, pass_on)
+        loop(0, per, lambda j: pass_on((g + 1) * per + j))
+
+    with jax.named_scope("later"):
+        loop(1, groups, later)
+    with jax.named_scope("passon"):
+        loop(1, per, lambda j: pass_on(per - j))
     _, acc = quad_sum(0)
     total[...] += acc
 
@@ -418,14 +526,15 @@
         line_copy(0, z, here.z).wait_recv()
         total[...] += line_buf[z].astype(F32)
 
-    loop(1, here.lines, add)
+    with jax.named_scope("addl"):
+        loop(1, here.lines, add)
     joined[:, :wide] = (resid1[...] + rms_scale(total[...], g3[...])).astype(BF16)
 
     for copy in swaps:
         copy.wait_send()
-    for plane in (first, second, third):
+    for plane in (first, third):
         plane.finish()
-    for plane in (q_outs, o_outs, tabs):
+    for plane in (q_outs, tabs):
         plane.others(plane.wait_sent)
 
     def sent(z):
@@ -433,6 +542,14 @@
             quad_copy(p, z).wait_send()
 
     loop(0, here.lines, sent)
+    for p in range(2):
+        quad_weight(p).wait_send()
+        relay_weight(p).wait_send()
+    for q in range(4):
+        pair_weight(q).wait_send()
+    for h in range(2):
+        loop(1, here.lines, lambda i: line_rows(i, h).wait_send())
+    loop(1, here.lines, lambda i: line_outs(i).wait_send())
     loop(1, here.lines, lambda i: line_copy(i, 0, here.z).wait_send())
 
 
@@ -460,22 +577,23 @@
         in_specs=[pl.BlockSpec(memory_space=pltpu.SMEM)] + [vm] * 8 + [hbm] * 12,
         out_specs=vm,
         scratch_shapes=[
-            half(seqs, wide), half(n, seqs, wide), half(seqs, wide), half(n, seqs, wide),
+            half(seqs, wide), half(n, seqs, wide), half(seqs, wide), half(lines, seqs, wide),
             half(seqs, wide), half(n, seqs, wide),
-            half(2 * own, wide), half(2 * own, wide), half(wide, 2 * own), half(wide, 2 * own),
+            half(2 * own, wide), half(wide, 2 * own), half(4, 2 * own, wide),
             half(*wk.shape), half(*wv.shape), half(*ck.shape), half(*cv.shape),
             half(LANES, 2 * LANES), full(seqs, pairs, LANES), full(seqs, pairs, LANES),
             half(n, seqs, 2 * own), half(n, seqs, 2 * own),
-            half(n, seqs, 2 * own), half(n, seqs, 2 * own),
+            half(lines, seqs, 8 * own), half(lines, seqs, 8 * own),
             full(seqs, wide), full(n, 2, LANES), full(n, 2, LANES), full(bias.shape[1], 1),
             half(2, wide, ff), half(2, wide, ff), half(2 * ff, wide),
             half(*sg.shape), half(*su.shape), half(*sd.shape),
             full(seqs, wide), half(n, seqs, wide), half(3, lines, seqs, wide),
             half(lines, seqs, wide), half(lines, seqs, wide),
-            sems((3, n)), sems((n,)), sems((3, n)), sems((n,)), sems((3, n)), sems((n,)),
-            sems((n,)), sems((n,)), sems((n,)), sems((n,)), sems((n,)), sems((n,)),
-            sems((5,)), sems((5,)), sems((3, lines)), sems((3, lines)),
-            sems((lines,)), sems((lines,)), sems((12,)),
+            sems((3, n)), sems((n,)), sems((2, lines)), sems((2, lines)), sems((3, n)), sems((n,)),
+            sems((n,)), sems((n,)), sems((lines,)), sems((lines,)), sems((n,)), sems((n,)),
+            sems((4,)), sems((4,)), sems((3, lines)), sems((3, lines)),
+            sems((lines,)), sems((lines,)), sems((2,)), sems((2,)), sems((2,)), sems((2,)),
+            sems((4,)), sems((4,)), sems((12,)),
         ],
         compiler_params=pltpu.CompilerParams(
             collective_id=0, has_side_effects=True, vmem_limit_bytes=62 << 20

time: 91.6 us -> 81.8 us (0.89)
  Pallas kernels: 90.7 us -> 80.9 us
    pallas_call x1, Pallas kernels: 89.2 us -> 79.4 us  [run_layer(): pl.pallas_call(functools.partial(layer_kernel, n), out_shape=jax.ShapeDty...]
where the time goes in v2:
time: 81.8 us; the launch traced here: 81.6 us
  Pallas kernels  80.9 us (99%)
    pallas_call x1, Pallas kernels, run_layer(): pl.pallas_call(functools.partial(layer_kernel, n), out_shape=jax.ShapeDty...  79.4 us

profile of v2, /device:TPU:0, one launch (start us, length us, event | category | flops | bytes accessed | tf_op | source)
XLA Modules:
  0.0 81.6 jit_solution(8063744797287154150)
XLA Ops:
  0.6 79.4 %shard_map.220.joined = bf16[16,2304]{1,0:T(8,128)(2,1)} custom-call(s32[16]{0:T(128)} %lens.1, bf16[16,2048]{1,0:T(8,128)(2,1)} %tok.1, f32[1,2048]{1,0:T(1,128)} %bitcast.11, f32[1,2048]{1,0:T(1,128)} %bitcast.12, f32[1,2048]{1,0:T(1,128)} %bitcast.13, f32[1,2048]{1,0:T(1,128)} %bitcast.14, f32[1,32]{1,0:T(1,128)} %bitcast.17, s32[6,16]{1,0:T(8,128)} %bitcast.15, ...), custom_call_target="tpu_custom_call" | custom-call | tf_op jit(solution)/shard_map/pallas_call | solution.py:574
  80.0 1.5 %shard_map.221 = (bf16[16,2048]{1,0:T(8,128)(2,1)}, bf16[16,128]{1,0:T(8,128)(2,1)}, bf16[16,128]{1,0:T(8,128)(2,1)}) custom-call(bf16[16,2304]{1,0:T(8,128)(2,1)} %shard_map.220.joined), custom_call_target="tpu_custom_call" | custom-call | tf_op jit(solution)/shard_map/pallas_call | solution.py:602
